TPU v7x, 32 devices: a whole 2x2x4 slice. The times are simulated.
32 devices in a mesh: dp: 4 (over y, x), kv: 4 (over z), tp: 2 (over core).
Axes of the slice: x: 2, y: 2, z: 4, core: 2. Of those that a mesh axis runs over, the one named last changes fastest.
Arguments:
- piece_tokens: bfloat16 [256, 2048], P(('dp', 'kv')), parts along dimension 0, may hold values from -6 to 6
- dec_tokens: bfloat16 [192, 4, 2048], P(('dp', 'kv')), parts along dimension 0, may hold values from -6 to 6
- norm_gain: float32 [2048], replicated, may hold values from 0.1 to 1.9
- query_weight: bfloat16 [2048, 1024], P(None, 'tp'), may hold values from -0.375 to 0.375
- key_weight: bfloat16 [2048, 256], P(None, 'tp'), may hold values from -0.125 to 0.125
- value_weight: bfloat16 [2048, 256], P(None, 'tp'), may hold values from -0.125 to 0.125
- gate_weight: bfloat16 [2048, 8], P(None, 'tp'), may hold values from -0.125 to 0.125
- gate_bias: float32 [8], P('tp'), may hold values from 3.4 to 11
- out_weight: bfloat16 [1024, 2048], P('tp'), may hold values from -0.1875 to 0.1875
- out_gain: float32 [2048], replicated, may hold values from 0.1 to 1.9
- past_keys: bfloat16 [4096, 2, 128], P(('dp', 'kv'), 'tp'), parts along dimension 0, may hold values from -41 to 41
- past_values: bfloat16 [4096, 2, 128], P(('dp', 'kv'), 'tp'), parts along dimension 0, may hold values from -6 to 6
- past_gate: float32 [8, 4096], P('tp', ('dp', 'kv')), parts along dimension 1, may hold values from -1024 to 0
- dec_keys: bfloat16 [192, 512, 2, 128], P(('dp', 'kv'), None, 'tp'), parts along dimension 0, may hold values from -41 to 41
- dec_values: bfloat16 [192, 512, 2, 128], P(('dp', 'kv'), None, 'tp'), parts along dimension 0, may hold values from -6 to 6
- dec_gate: float32 [192, 8, 512], P(('dp', 'kv'), 'tp'), parts along dimension 0, may hold values from -512 to 0
- dec_lengths: int32 [192], P(('dp', 'kv')), parts along dimension 0, may hold values from 1 to 512, as said below
Outputs:
- piece_out: bfloat16 [256, 2048], P(('dp', 'kv')), parts along dimension 0
- dec_out: bfloat16 [192, 4, 2048], P(('dp', 'kv')), parts along dimension 0
There are 4 independent parts, one for each index of `dp`. A program takes and returns all parts, laid end to end along the dimension named above; an argument that names none is the same for every part. Nothing has to cross between parts.
Inputs may be any that keep to these rules, and one draw needn't show every extreme that they name: `dec_lengths`: some decoding sequence has all 512 slots live in every draw.
All inputs are finite; a program needn't handle non-finite values.
Results may differ from a plain program's by a relative error of at most 0.015.
Values may be sent and summed in bfloat16 or wider, within the bound.
A program may use at most 64 MiB of HBM per device.

v0:
```python
import jax
import jax.numpy as jnp
from jax import lax
from jax.sharding import PartitionSpec as P

EPS = 1e-06


def rms_scale(source, scale_gain):
    widened = source.astype(jnp.float32)
    return (
        widened * lax.rsqrt(jnp.mean(widened * widened, axis=-1, keepdims=True) + EPS) * scale_gain
    )


def body(
    piece_tokens,
    dec_tokens,
    norm_gain,
    query_weight,
    key_weight,
    value_weight,
    gate_weight,
    gate_bias,
    out_weight,
    out_gain,
    past_keys,
    past_values,
    past_gate,
    dec_keys,
    dec_values,
    dec_gate,
    dec_lengths,
):
    piece_rows = piece_tokens.shape[0]
    model_width = piece_tokens.shape[1]
    kv_local = past_keys.shape[1]
    head_dim = past_keys.shape[2]
    heads_local = gate_bias.shape[0]
    group_size = heads_local // kv_local
    score_scale = head_dim ** (-0.5)
    seq_count = dec_tokens.shape[0]
    new_count = dec_tokens.shape[1]
    kv_count = lax.axis_size("kv")
    position = lax.axis_index("kv")
    all_rows = jnp.concatenate(
        [piece_tokens, dec_tokens.reshape(seq_count * new_count, model_width)], axis=0
    )
    normed = rms_scale(all_rows, norm_gain).astype(jnp.bfloat16)
    queries = jnp.dot(normed, query_weight, preferred_element_type=jnp.float32).astype(jnp.bfloat16)
    key_rows = jnp.dot(normed, key_weight, preferred_element_type=jnp.float32).astype(jnp.bfloat16)
    value_rows = jnp.dot(normed, value_weight, preferred_element_type=jnp.float32).astype(
        jnp.bfloat16
    )
    log_gates = jax.nn.log_sigmoid(
        jnp.dot(normed, gate_weight, preferred_element_type=jnp.float32) + gate_bias
    )
    piece_queries = queries[:piece_rows]
    piece_keys = key_rows[:piece_rows].reshape(piece_rows, kv_local, head_dim)
    piece_values = value_rows[:piece_rows].reshape(piece_rows, kv_local, head_dim)
    local_run = jnp.cumsum(log_gates[:piece_rows], axis=0)
    gathered_run = lax.all_gather(local_run, "kv", axis=0, tiled=True)
    shard_run = gathered_run.reshape(kv_count, piece_rows, heads_local)
    totals = shard_run[:, -1]
    before = jnp.cumsum(totals, axis=0) - totals
    piece_run = (shard_run + before[:, None, :]).reshape(kv_count * piece_rows, heads_local)
    own_run = lax.dynamic_slice_in_dim(piece_run, position * piece_rows, piece_rows, 0)
    key_place = position * piece_rows + jnp.arange(piece_rows)
    gate_groups = jnp.moveaxis(past_gate.reshape(kv_local, group_size, -1), 1, 0)
    own_groups = jnp.moveaxis(own_run.reshape(piece_rows, kv_local, group_size), 2, 0)
    shard_queries = lax.all_gather(piece_queries, "kv", axis=0, tiled=True)
    row_count = shard_queries.shape[0]
    query_groups = jnp.moveaxis(
        shard_queries.reshape(row_count, kv_local, group_size, head_dim), 2, 0
    )
    run_groups = jnp.moveaxis(piece_run.reshape(row_count, kv_local, group_size), 2, 0)
    row_place = jnp.arange(row_count)
    causal = key_place[None, :] <= row_place[:, None]

    def one_group(inputs):
        query_one, run_one, gate_one, key_run_one = inputs
        row_bias = run_one.T[:, :, None]
        past_scores = (
            jnp.einsum("nkd,pkd->knp", query_one, past_keys, preferred_element_type=jnp.float32)
            * score_scale
        )
        past_scores = past_scores + gate_one[:, None, :] + row_bias
        new_scores = (
            jnp.einsum("nkd,jkd->knj", query_one, piece_keys, preferred_element_type=jnp.float32)
            * score_scale
        )
        new_scores = new_scores + row_bias - key_run_one.T[:, None, :]
        new_scores = jnp.where(causal[None], new_scores, -jnp.inf)
        row_top = jnp.maximum(jnp.max(past_scores, axis=-1), jnp.max(new_scores, axis=-1))
        past_exp = jnp.exp(past_scores - row_top[..., None])
        new_exp = jnp.exp(new_scores - row_top[..., None])
        row_total = jnp.sum(past_exp, axis=-1) + jnp.sum(new_exp, axis=-1)
        summed = jnp.einsum(
            "knp,pkd->nkd",
            past_exp.astype(jnp.bfloat16),
            past_values,
            preferred_element_type=jnp.float32,
        )
        summed = summed + jnp.einsum(
            "knj,jkd->nkd",
            new_exp.astype(jnp.bfloat16),
            piece_values,
            preferred_element_type=jnp.float32,
        )
        return (summed, row_top.T, row_total.T)

    group_out, group_top, group_total = lax.map(
        one_group, (query_groups, run_groups, gate_groups, own_groups)
    )
    group_out = jnp.moveaxis(group_out, 0, 2).reshape(row_count, heads_local, head_dim)
    group_top = jnp.moveaxis(group_top, 0, 2).reshape(row_count, heads_local)
    group_total = jnp.moveaxis(group_total, 0, 2).reshape(row_count, heads_local)
    arrived = (
        lax.all_to_all(
            group_out.reshape(kv_count, piece_rows, heads_local, head_dim),
            "kv",
            split_axis=0,
            concat_axis=0,
            tiled=True,
        ),
        lax.all_to_all(
            group_top.reshape(kv_count, piece_rows, heads_local),
            "kv",
            split_axis=0,
            concat_axis=0,
            tiled=True,
        ),
        lax.all_to_all(
            group_total.reshape(kv_count, piece_rows, heads_local),
            "kv",
            split_axis=0,
            concat_axis=0,
            tiled=True,
        ),
    )
    global_top = jnp.max(arrived[1], axis=0)
    weights = jnp.exp(arrived[1] - global_top)
    row_total = jnp.sum(arrived[2] * weights, axis=0)
    piece_result = jnp.sum(arrived[0] * weights[..., None], axis=0) / row_total[..., None]
    piece_attention = piece_result.reshape(piece_rows, heads_local * head_dim).astype(jnp.bfloat16)
    dec_queries = queries[piece_rows:].reshape(seq_count, new_count, kv_local, group_size, head_dim)
    dec_new_keys = key_rows[piece_rows:].reshape(seq_count, new_count, kv_local, head_dim)
    dec_new_values = value_rows[piece_rows:].reshape(seq_count, new_count, kv_local, head_dim)
    dec_run = jnp.cumsum(log_gates[piece_rows:].reshape(seq_count, new_count, heads_local), axis=1)
    past_len = dec_keys.shape[1]
    slot_index = jnp.arange(past_len)
    last_gate = jnp.sum(
        jnp.where(slot_index[None, None, :] == (dec_lengths - 1)[:, None, None], dec_gate, 0.0),
        axis=2,
    )
    query_bias = jnp.moveaxis(dec_run.reshape(seq_count, new_count, kv_local, group_size), 1, 3)
    past_bias = last_gate.reshape(seq_count, kv_local, group_size)[..., None, None]
    dec_gate_groups = dec_gate.reshape(seq_count, kv_local, group_size, past_len)
    new_scores = (
        jnp.einsum(
            "stkgd,sukd->skgtu", dec_queries, dec_new_keys, preferred_element_type=jnp.float32
        )
        * score_scale
    )
    new_scores = new_scores + query_bias[..., None] - query_bias[..., None, :]
    new_causal = jnp.arange(new_count)[None, :] <= jnp.arange(new_count)[:, None]
    new_scores = jnp.where(new_causal, new_scores, -jnp.inf)
    new_top = jnp.max(new_scores, axis=-1)
    new_exp = jnp.exp(new_scores - new_top[..., None])
    start_dec = (
        jnp.einsum(
            "skgtu,sukd->skgtd",
            new_exp.astype(jnp.bfloat16),
            dec_new_values,
            preferred_element_type=jnp.float32,
        ),
        new_top,
        jnp.sum(new_exp, axis=-1),
    )
    block_scores = (
        jnp.einsum("stkgd,spkd->skgtp", dec_queries, dec_keys, preferred_element_type=jnp.float32)
        * score_scale
    )
    block_scores = (
        block_scores + query_bias[..., None] + past_bias - dec_gate_groups[:, :, :, None, :]
    )
    live_mask = jnp.arange(past_len)[None, :] < dec_lengths[:, None]
    block_scores = jnp.where(live_mask[:, None, None, None, :], block_scores, -jnp.inf)
    row_top = jnp.maximum(start_dec[1], jnp.max(block_scores, axis=-1))
    block_exp = jnp.exp(block_scores - row_top[..., None])
    rescale = jnp.exp(start_dec[1] - row_top)
    summed = start_dec[0] * rescale[..., None] + jnp.einsum(
        "skgtp,spkd->skgtd",
        block_exp.astype(jnp.bfloat16),
        dec_values,
        preferred_element_type=jnp.float32,
    )
    dec_attention = summed / (start_dec[2] * rescale + jnp.sum(block_exp, axis=-1))[..., None]
    dec_attention = (
        jnp.transpose(dec_attention, (0, 3, 1, 2, 4))
        .reshape(seq_count * new_count, heads_local * head_dim)
        .astype(jnp.bfloat16)
    )
    attention = jnp.concatenate([piece_attention, dec_attention], axis=0)
    partial_rows = jnp.dot(attention, out_weight, preferred_element_type=jnp.float32)
    mixed = lax.psum(partial_rows.astype(jnp.bfloat16), "tp").astype(jnp.float32)
    final_rows = rms_scale(mixed, out_gain).astype(jnp.bfloat16)
    return (
        final_rows[:piece_rows],
        final_rows[piece_rows:].reshape(seq_count, new_count, model_width),
    )


def solution(mesh):
    return jax.shard_map(
        body,
        mesh=mesh,
        in_specs=(
            P(("dp", "kv"), None),
            P(("dp", "kv"), None, None),
            P(),
            P(None, "tp"),
            P(None, "tp"),
            P(None, "tp"),
            P(None, "tp"),
            P("tp"),
            P("tp", None),
            P(),
            P(("dp", "kv"), "tp", None),
            P(("dp", "kv"), "tp", None),
            P("tp", ("dp", "kv")),
            P(("dp", "kv"), None, "tp", None),
            P(("dp", "kv"), None, "tp", None),
            P(("dp", "kv"), "tp", None),
            P(("dp", "kv")),
        ),
        out_specs=(P(("dp", "kv"), None), P(("dp", "kv"), None, None)),
        check_vma=False,
    )
```

profile of v0, /device:TPU:0, one launch (start us, length us, event | category | flops | bytes accessed | tf_op | source)
XLA Modules:
  0.0 105.0 jit_solution(5508176570152350641)
XLA Ops:
  7.2 1.1 %reshape.318 = bf16[48,2048]{1,0:T(8,128)(2,1)S(1)} reshape(bf16[12,4,2048]{2,1,0:T(4,128)(2,1)} %param.20) | data formatting | bytes 393216 | tf_op jit(solution)/shard_map/reshape | solution.py:47
  8.4 1.0 fusion.69
  9.4 1.1 %fusion.87 = f32[64,4]{0,1:T(4,128)S(1)} fusion(bf16[2048,4]{0,1:T(4,128)(2,1)} %param.25, f32[4]{0:T(128)} %param.26, f32[2048]{0:T(1024)} %param.21, f32[64]{0:T(128)S(1)} %add_rsqrt_fusion.1, bf16[48,2048]{1,0:T(8,128)(2,1)S(1)} %reshape.318, bf16[16,2048]{1,0:T(8,128)(2,1)} %param.19), kind=kOutput, calls=%fused_computation.106 | convolution fusion | flops 1968384 | bytes 288016 | tf_op jit(solution)/shard_map/dot_general | solution.py:56
  10.7 13.6 %all-gather = f32[4,16,4]{1,2,0:T(4,128)S(1)} all-gather(f32[1,16,4]{1,2,0:T(4,128)S(1)} %bitcast.224), channel_id=1, replica_groups=mesh['dp'=4,'kv'=4,'tp'=2] {'kv'}, dimensions={0}, use_global_device_ids=true | all-gather | bytes 1280 | tf_op jit(solution)/shard_map/all_gather | solution.py:62
  24.8 0.9 transpose_reshape.3
  25.6 1.4 %convolution_convert_fusion.3 = bf16[64,128]{1,0:T(8,128)(2,1)S(1)} fusion(bf16[2048,128]{1,0:T(8,128)(2,1)} %param.23, f32[2048]{0:T(1024)} %param.21, f32[64]{0:T(128)S(1)} %add_rsqrt_fusion.1, bf16[48,2048]{1,0:T(8,128)(2,1)S(1)} %reshape.318, bf16[16,2048]{1,0:T(8,128)(2,1)} %param.19), kind=kOutput, calls=%fused_computation.61 | convolution fusion | flops 34480128 | bytes 811264 | tf_op jit(solution)/shard_map/dot_general | solution.py:51
  27.1 0.3 convolution_convert_fusion.2
  27.4 0.5 convolution_convert_fusion.1
  27.9 13.1 %all_gather.6 = bf16[64,512]{1,0:T(8,128)(2,1)S(1)} all-gather(bf16[16,512]{1,0:T(8,128)(2,1)S(1)} %slice.44), channel_id=1, replica_groups=mesh['dp'=4,'kv'=4,'tp'=2] {'kv'}, dimensions={0}, use_global_device_ids=true | all-gather | bytes 81920 | tf_op jit(solution)/shard_map/all_gather | solution.py:71
  41.2 4.4 %while.15 = (s32[]{:T(128)}, f32[4,64,1,128]{3,1,2,0:T(8,128)S(1)}, f32[4,64,1]{1,2,0:T(1,128)S(1)}, f32[4,64,1]{1,2,0:T(1,128)S(1)}, bf16[4,64,1,128]{3,1,2,0:T...) while((s32[]{:T(128)}, f32[4,64,1,128]{3,1,2,0:T(8,128)S(1)}, ...), condition=%wide.region_8.9_spmd.clone, body=%wide.region_3.8_spmd.clone.sunk | while | flops 9062274 | bytes 495149 | solution.py:112
  41.4 0.3 fusion.126
  42.5 0.3 fusion.126
  45.7 0.6 copy.73
  46.3 3.4 %all-to-all-start.1 = ((f32[4,16,4]{1,2,0:T(4,128)}), f32[4,16,4]{1,2,0:T(4,128)S(1)}, u32[]{:S(2)}, u32[]{:S(2)}) async-start(f32[4,16,4]{1,2,0:T(4,128)} %copy.73), calls=%async_computation.1 | async-start | bytes 16384 | tf_op jit(solution)/shard_map/all_to_all | solution.py:126
  50.1 0.6 reduce_window_sum.38
  50.9 0.6 fusion.95
  51.6 0.4 copy.80
  52.1 2.0 %fusion.96 = (f32[12,4,4]{1,2,0:T(4,128)S(1)}, f32[12,1,4,4,512]{4,2,3,0,1:T(4,128)S(1)}) fusion(f32[12,4,512]{2,1,0:T(4,128)S(1)} %copy-done.5, f32[12,4]{1,0:T(8,128)S(1)} %select_reduce_fusion, f32[12,4,4]{1,2,0:T(4,128)S(1)} %copy.78, bf16[12,4,4,128]{3,2,1,0:T(4,128)(2,1)S(1)} %reshape.325, bf16[12,512,1,128]{3,1,2,0:T(8,128)(2,1)} %param.32, ...), kind=kOutput, calls=%fused_computation.119 | convolution fusion | flops 25755456 | bytes 2121408 | tf_op jit(solution)/shard_map/stkgd,spkd->skgtp/dot_general | solution.py:181
  54.2 0.3 fusion.77
  54.9 0.6 copy.75
  55.7 5.1 %all-to-all-start.2 = ((f32[4,16,4]{1,2,0:T(4,128)}), f32[4,16,4]{1,2,0:T(4,128)S(1)}, u32[]{:S(2)}, u32[]{:S(2)}) async-start(f32[4,16,4]{1,2,0:T(4,128)} %copy.75), calls=%async_computation.2 | async-start | bytes 16384 | tf_op jit(solution)/shard_map/all_to_all | solution.py:133
  60.8 1.8 %fusion.65 = bf16[12,4,1,4,128]{4,1,3,0,2:T(4,128)(2,1)S(1)} fusion(f32[12,4,4,128]{3,2,1,0:T(4,128)S(1)} %convolution_multiply_fusion.2, bf16[12,512,1,128]{3,1,2,0:T(8,128)(2,1)} %param.33, bf16[12,4,4,512]{3,1,2,0:T(4,128)(2,1)S(1)} %get-tuple-element.191, f32[12,4,4]{2,1,0:T(4,128)S(1)} %copy.84), kind=kOutput, calls=%fused_computation.59 | convolution fusion | flops 25239552 | bytes 1917696 | tf_op jit(solution)/shard_map/skgtp,spkd->skgtd/dot_general | solution.py:192
  62.6 0.7 copy.72
  63.3 3.2 %all-to-all-done.2 = f32[4,16,4]{1,2,0:T(4,128)S(1)} async-done(((f32[4,16,4]{1,2,0:T(4,128)}), f32[4,16,4]{1,2,0:T(4,128)S(1)}, u32[]{:S(2)}, u32[]{:S(2)}) %all-to-all-start.2) | async-done | bytes 1056 | tf_op jit(solution)/shard_map/all_to_all | solution.py:133
  66.5 3.3 %all-to-all-start = ((f32[4,16,4,128]{3,1,2,0:T(8,128)}), f32[4,16,4,128]{3,1,2,0:T(8,128)S(1)}, u32[]{:S(2)}, u32[]{:S(2)}) async-start(f32[4,16,4,128]{3,1,2,0:T(8,128)} %copy.72), calls=%async_computation | async-start | bytes 262144 | tf_op jit(solution)/shard_map/all_to_all | solution.py:119
  69.9 5.8 %all-to-all-done = f32[4,16,4,128]{3,1,2,0:T(8,128)S(1)} async-done(((f32[4,16,4,128]{3,1,2,0:T(8,128)}), f32[4,16,4,128]{3,1,2,0:T(8,128)S(1)}, u32[]{:S(2)}, u32[]{:S(2)}) %all-to-all-start) | async-done | bytes 131104 | tf_op jit(solution)/shard_map/all_to_all | solution.py:119
  75.9 1.2 %convolution_convert_fusion = bf16[64,2048]{1,0:T(8,128)(2,1)} fusion(bf16[512,2048]{1,0:T(8,128)(2,1)S(1)} %copy-done, bf16[48,512]{1,0:T(8,128)(2,1)S(1)} %bitcast.214, bf16[16,512]{1,0:T(8,128)(2,1)S(1)} %copy_bitcast_fusion.2), kind=kOutput, calls=%fused_computation.38 | convolution fusion | flops 134479872 | bytes 2424832 | tf_op jit(solution)/shard_map/dot_general | solution.py:205
  77.1 17.4 %all-reduce.2.cloned.1.call-done = bf16[64,2048]{1,0:T(8,128)(2,1)} async-done(((bf16[64,2048]{1,0:T(8,128)(2,1)}), bf16[64,2048]{1,0:T(8,128)(2,1)}) %all-reduce.2.cloned.1.call-update) | async-done | bytes 262160 | tf_op jit(solution)/shard_map/psum | solution.py:206
  94.6 1.1 %fusion.72 = f32[64]{0:T(128)S(1)} fusion(bf16[64,2048]{1,0:T(8,128)(2,1)} %all-reduce.2.cloned.1.call-done), kind=kLoop, calls=%fused_computation.72 | loop fusion | flops 393152 | bytes 262400 | tf_op jit(solution)/shard_map/reduce_sum | solution.py:12
  95.7 1.1 %fusion.74 = bf16[64,2048]{1,0:T(8,128)(2,1)S(1)} fusion(bf16[64,2048]{1,0:T(8,128)(2,1)} %all-reduce.2.cloned.1.call-done, f32[2048]{0:T(1024)S(1)} %copy-done.8, f32[64]{0:T(128)S(1)} %add_rsqrt_fusion), kind=kLoop, calls=%fused_computation.74 | loop fusion | flops 524288 | bytes 532736 | tf_op jit(solution)/shard_map/convert_element_type | solution.py:207
  96.8 0.6 slice.51
  97.4 0.8 reshape.331
  (116 shorter events, 6.2 us)
Async XLA Ops:
  7.2 68.7 %copy-start = (bf16[512,2048]{1,0:T(8,128)(2,1)S(1)}, bf16[512,2048]{1,0:T(8,128)(2,1)}, u32[]{:S(2)}) copy-start(bf16[512,2048]{1,0:T(8,128)(2,1)} %param.27) | copy-start | bytes 6291460
  7.2 19.8 %copy-start.4 = (bf16[16,2048]{1,0:T(8,128)(2,1)S(1)}, bf16[16,2048]{1,0:T(8,128)(2,1)}, u32[]{:S(2)}) copy-start(bf16[16,2048]{1,0:T(8,128)(2,1)} %param.19) | copy-start | bytes 196612
  7.2 19.8 %copy-start.7 = (f32[2048]{0:T(1024)S(1)}, f32[2048]{0:T(1024)}, u32[]{:S(2)}) copy-start(f32[2048]{0:T(1024)} %param.21) | copy-start | bytes 24580
  7.2 19.8 %copy-start.10 = (bf16[2048,128]{1,0:T(8,128)(2,1)S(1)}, bf16[2048,128]{1,0:T(8,128)(2,1)}, u32[]{:S(2)}) copy-start(bf16[2048,128]{1,0:T(8,128)(2,1)} %param.24) | copy-start | bytes 1572868
  24.8 2.6 %copy-start.1 = (bf16[2048,512]{1,0:T(8,128)(2,1)S(1)}, bf16[2048,512]{1,0:T(8,128)(2,1)}, u32[]{:S(2)}) copy-start(bf16[2048,512]{1,0:T(8,128)(2,1)} %param.22) | copy-start | bytes 6291460
  27.0 14.2 %copy-start.2 = (bf16[256,1,128]{2,0,1:T(8,128)(2,1)S(1)}, bf16[256,1,128]{2,0,1:T(8,128)(2,1)}, u32[]{:S(2)}) copy-start(bf16[256,1,128]{2,0,1:T(8,128)(2,1)} %param.29) | copy-start | bytes 196612
  27.0 14.2 %copy-start.3 = (bf16[256,1,128]{2,0,1:T(8,128)(2,1)S(1)}, bf16[256,1,128]{2,0,1:T(8,128)(2,1)}, u32[]{:S(2)}) copy-start(bf16[256,1,128]{2,0,1:T(8,128)(2,1)} %param.30) | copy-start | bytes 196612
  27.4 22.5 %copy-start.6 = (bf16[64,128]{1,0:T(8,128)(2,1)}, bf16[64,128]{1,0:T(8,128)(2,1)S(1)}, u32[]{:S(2)}) copy-start(bf16[64,128]{1,0:T(8,128)(2,1)S(1)} %convolution_convert_fusion.2) | copy-start | bytes 49156
  27.9 21.8 %copy-start.9 = (s32[12]{0:T(128)S(1)}, s32[12]{0:T(128)}, u32[]{:S(2)}) copy-start(s32[12]{0:T(128)} %param.35) | copy-start | bytes 148
  41.2 10.8 %copy-start.5 = (f32[12,4,512]{2,1,0:T(4,128)S(1)}, f32[12,4,512]{2,1,0:T(4,128)}, u32[]{:S(2)}) copy-start(f32[12,4,512]{2,1,0:T(4,128)} %param.34) | copy-start | bytes 294916
  46.3 9.4 %all-to-all-start.1 = ((f32[4,16,4]{1,2,0:T(4,128)}), f32[4,16,4]{1,2,0:T(4,128)S(1)}, u32[]{:S(2)}, u32[]{:S(2)}) async-start(f32[4,16,4]{1,2,0:T(4,128)} %copy.73), calls=%async_computation.1 | async-start | bytes 16384 | tf_op jit(solution)/shard_map/all_to_all | solution.py:126
  50.1 4.6 %slice-start = ((bf16[64,128]{1,0:T(8,128)(2,1)}), bf16[48,128]{1,0:T(8,128)(2,1)S(1)}, s32[]{:S(2)}) async-start(bf16[64,128]{1,0:T(8,128)(2,1)} %copy-done.6), calls=%async_computation.4 | async-start | bytes 24576 | tf_op jit(solution)/shard_map/slice | solution.py:148
  55.7 10.8 %all-to-all-start.2 = ((f32[4,16,4]{1,2,0:T(4,128)}), f32[4,16,4]{1,2,0:T(4,128)S(1)}, u32[]{:S(2)}, u32[]{:S(2)}) async-start(f32[4,16,4]{1,2,0:T(4,128)} %copy.75), calls=%async_computation.2 | async-start | bytes 16384 | tf_op jit(solution)/shard_map/all_to_all | solution.py:133
  62.6 33.1 %copy-start.8 = (f32[2048]{0:T(1024)S(1)}, f32[2048]{0:T(1024)}, u32[]{:S(2)}) copy-start(f32[2048]{0:T(1024)} %param.28) | copy-start | bytes 24580
  66.5 9.2 %all-to-all-start = ((f32[4,16,4,128]{3,1,2,0:T(8,128)}), f32[4,16,4,128]{3,1,2,0:T(8,128)S(1)}, u32[]{:S(2)}, u32[]{:S(2)}) async-start(f32[4,16,4,128]{3,1,2,0:T(8,128)} %copy.72), calls=%async_computation | async-start | bytes 262144 | tf_op jit(solution)/shard_map/all_to_all | solution.py:119
  69.8 24.7 %all-reduce.2.cloned.1.call-start = ((), (), s32[]{:S(2)}) async-start(), calls=%async_computation.3 | async-start | bytes 524288 | tf_op jit(solution)/shard_map/psum | solution.py:206
Sparse Core Ops, SparseCore 0:
  77.2 17.2 all-reduce.1
where the time goes:
time: 106 us; the launch traced here: 105 us
  blocking collectives  26.8 us (25%)
  waiting for transfers between devices  26.5 us (25%)
  between operations  14.4 us (14%)
  matrix products  12.2 us (12%)
  starting transfers between devices  11.9 us (11%)
  local copies, waits for them, and re-layouts  7.15 us (7%)
  other arithmetic  6.01 us (6%)
    psum x1, waiting for transfers between devices, body(): lax.psum(partial_rows.astype(jnp.bfloat16), 'tp').astype(jnp.float32)  17.4 us
    all_gather x1, blocking collectives, body(): gathered_run = lax.all_gather(local_run, 'kv', axis=0, tiled=True)  13.6 us
    all_gather x1, blocking collectives, body(): shard_queries = lax.all_gather(piece_queries, 'kv', axis=0, tiled=True)  13.1 us
    all_to_all x1, waiting for transfers between devices, body(): lax.all_to_all(group_out.reshape(kv_count, piece_rows, heads_local, head_...  5.81 us
    all_to_all x1, starting transfers between devices, body(): lax.all_to_all(group_total.reshape(kv_count, piece_rows, heads_local), 'k...  5.09 us
    all_to_all x1, starting transfers between devices, body(): lax.all_to_all(group_top.reshape(kv_count, piece_rows, heads_local), 'kv'...  3.44 us
    all_to_all x1, starting transfers between devices, body(): lax.all_to_all(group_out.reshape(kv_count, piece_rows, heads_local, head_...  3.33 us
    all_to_all x1, waiting for transfers between devices, body(): lax.all_to_all(group_total.reshape(kv_count, piece_rows, heads_local), 'k...  3.19 us
  transfers between devices with their start and end apart: 4, of which 3 were waited for; matrix products, arithmetic and copies ran while one was open for 8% of the time, Pallas kernels for 0%

commit v1 on v0

--- a/solution.py
+++ b/solution.py
@@ -4,6 +4,12 @@
 from jax.sharding import PartitionSpec as P
 
 EPS = 1e-06
+
+
+def summed_here(shard, axis):
+    parts = lax.all_gather(shard, axis, axis=0, tiled=False)
+    total = parts.sum(axis=0)
+    return total
 
 
 def rms_scale(source, scale_gain):
@@ -203,7 +209,7 @@
     )
     attention = jnp.concatenate([piece_attention, dec_attention], axis=0)
     partial_rows = jnp.dot(attention, out_weight, preferred_element_type=jnp.float32)
-    mixed = lax.psum(partial_rows.astype(jnp.bfloat16), "tp").astype(jnp.float32)
+    mixed = summed_here(partial_rows.astype(jnp.bfloat16), "tp").astype(jnp.float32)
     final_rows = rms_scale(mixed, out_gain).astype(jnp.bfloat16)
     return (
         final_rows[:piece_rows],

time: 106 us -> 74.5 us (0.70)
  waiting for transfers between devices: 26.5 us -> 9.07 us
  between operations: 14.4 us -> 0.99 us
  blocking collectives: 26.8 us -> 28.9 us
  other arithmetic: 6.01 us -> 4.24 us
    psum x1 -> x0, waiting for transfers between devices: 17.4 us -> none  [body(): lax.psum(partial_rows.astype(jnp.bfloat16), 'tp').astype(jnp.float32)]
    all_gather x0 -> x1, blocking collectives: none -> 2.18 us  [summed_here(): parts = lax.all_gather(shard, axis, axis=0, tiled=False)]
  transfers between devices with their start and end apart: 4 -> 3, of which waited for: 3 -> 2; matrix products, arithmetic and copies ran while one was open for 8% -> 11% of each run, Pallas kernels for 0% -> 0%
where the time goes in v1:
time: 74.5 us; the launch traced here: 73.9 us
  blocking collectives  28.9 us (39%)
  starting transfers between devices  11.9 us (16%)
  matrix products  11.5 us (15%)
  waiting for transfers between devices  9.07 us (12%)
  local copies, waits for them, and re-layouts  7.16 us (10%)
  other arithmetic  4.24 us (6%)
  between operations  0.99 us (1%)
    all_gather x1, blocking collectives, body(): gathered_run = lax.all_gather(local_run, 'kv', axis=0, tiled=True)  13.6 us
    all_gather x1, blocking collectives, body(): shard_queries = lax.all_gather(piece_queries, 'kv', axis=0, tiled=True)  13.1 us
    all_to_all x1, waiting for transfers between devices, body(): lax.all_to_all(group_out.reshape(kv_count, piece_rows, heads_local, head_...  5.86 us
    all_to_all x1, starting transfers between devices, body(): lax.all_to_all(group_total.reshape(kv_count, piece_rows, heads_local), 'k...  5.09 us
    all_to_all x1, starting transfers between devices, body(): lax.all_to_all(group_top.reshape(kv_count, piece_rows, heads_local), 'kv'...  3.44 us
    all_to_all x1, starting transfers between devices, body(): lax.all_to_all(group_out.reshape(kv_count, piece_rows, heads_local, head_...  3.33 us
    all_to_all x1, waiting for transfers between devices, body(): lax.all_to_all(group_total.reshape(kv_count, piece_rows, heads_local), 'k...  3.2 us
    all_gather x1, blocking collectives, summed_here(): parts = lax.all_gather(shard, axis, axis=0, tiled=False)  2.18 us
  transfers between devices with their start and end apart: 3, of which 2 were waited for; matrix products, arithmetic and copies ran while one was open for 11% of the time, Pallas kernels for 0%

profile of v1, /device:TPU:0, one launch (start us, length us, event | category | flops | bytes accessed | tf_op | source)
XLA Modules:
  0.0 73.9 jit_solution(9545910285803503520)
XLA Ops:
  0.7 1.1 %reshape.318 = bf16[48,2048]{1,0:T(8,128)(2,1)S(1)} reshape(bf16[12,4,2048]{2,1,0:T(4,128)(2,1)} %param.20) | data formatting | bytes 393216 | tf_op jit(solution)/shard_map/reshape | solution.py:53
  1.8 1.0 %fusion.69 = f32[64]{0:T(128)S(1)} fusion(bf16[48,2048]{1,0:T(8,128)(2,1)S(1)} %reshape.318, bf16[16,2048]{1,0:T(8,128)(2,1)} %param.19), kind=kLoop, calls=%fused_computation.69 | loop fusion | flops 786368 | bytes 262400 | tf_op jit(solution)/shard_map/reduce_sum | solution.py:18
  2.9 1.1 %fusion.87 = f32[64,4]{0,1:T(4,128)S(1)} fusion(bf16[2048,4]{0,1:T(4,128)(2,1)} %param.25, f32[4]{0:T(128)} %param.26, f32[2048]{0:T(1024)} %param.21, f32[64]{0:T(128)S(1)} %add_rsqrt_fusion.1, bf16[48,2048]{1,0:T(8,128)(2,1)S(1)} %reshape.318, bf16[16,2048]{1,0:T(8,128)(2,1)} %param.19), kind=kOutput, calls=%fused_computation.106 | convolution fusion | flops 1968384 | bytes 288016 | tf_op jit(solution)/shard_map/dot_general | solution.py:62
  4.2 13.6 %all-gather.1 = f32[4,16,4]{1,2,0:T(4,128)S(1)} all-gather(f32[1,16,4]{1,2,0:T(4,128)S(1)} %bitcast.226), channel_id=1, replica_groups=mesh['dp'=4,'kv'=4,'tp'=2] {'kv'}, dimensions={0}, use_global_device_ids=true | all-gather | bytes 1280 | tf_op jit(solution)/shard_map/all_gather | solution.py:68
  18.2 0.9 %transpose_reshape.3 = f32[4,1,256]{2,1,0:T(1,128)S(1)} reshape(f32[4,256]{1,0:T(4,128)} %param.31) | data formatting | bytes 8192 | tf_op jit(solution)/shard_map/transpose;reshape | solution.py:75
  19.1 1.4 %convolution_convert_fusion.3 = bf16[64,128]{1,0:T(8,128)(2,1)S(1)} fusion(bf16[2048,128]{1,0:T(8,128)(2,1)} %param.23, f32[2048]{0:T(1024)} %param.21, f32[64]{0:T(128)S(1)} %add_rsqrt_fusion.1, bf16[48,2048]{1,0:T(8,128)(2,1)S(1)} %reshape.318, bf16[16,2048]{1,0:T(8,128)(2,1)} %param.19), kind=kOutput, calls=%fused_computation.61 | convolution fusion | flops 34480128 | bytes 811264 | tf_op jit(solution)/shard_map/dot_general | solution.py:57
  20.5 0.3 convolution_convert_fusion.2
  20.8 0.5 convolution_convert_fusion.1
  21.4 13.1 %all_gather.12 = bf16[64,512]{1,0:T(8,128)(2,1)S(1)} all-gather(bf16[16,512]{1,0:T(8,128)(2,1)S(1)} %slice.44), channel_id=1, replica_groups=mesh['dp'=4,'kv'=4,'tp'=2] {'kv'}, dimensions={0}, use_global_device_ids=true | all-gather | bytes 81920 | tf_op jit(solution)/shard_map/all_gather | solution.py:77
  34.6 4.4 %while.15 = (s32[]{:T(128)}, f32[4,64,1,128]{3,1,2,0:T(8,128)S(1)}, f32[4,64,1]{1,2,0:T(1,128)S(1)}, f32[4,64,1]{1,2,0:T(1,128)S(1)}, bf16[4,64,1,128]{3,1,2,0:T...) while((s32[]{:T(128)}, f32[4,64,1,128]{3,1,2,0:T(8,128)S(1)}, ...), condition=%wide.region_8.9_spmd.clone, body=%wide.region_3.8_spmd.clone.sunk | while | flops 9062274 | bytes 495149 | solution.py:118
  34.8 0.3 fusion.126
  35.9 0.3 fusion.126
  37.0 0.3 fusion.126
  38.1 0.3 fusion.126
  39.1 0.6 copy.73
  39.7 3.4 %all-to-all-start.1 = ((f32[4,16,4]{1,2,0:T(4,128)}), f32[4,16,4]{1,2,0:T(4,128)S(1)}, u32[]{:S(2)}, u32[]{:S(2)}) async-start(f32[4,16,4]{1,2,0:T(4,128)} %copy.73), calls=%async_computation.1 | async-start | bytes 16384 | tf_op jit(solution)/shard_map/all_to_all | solution.py:132
  43.6 0.6 reduce_window_sum.38
  44.4 0.6 fusion.95
  45.1 0.4 copy.80
  45.6 2.0 %fusion.96 = (f32[12,4,4]{1,2,0:T(4,128)S(1)}, f32[12,1,4,4,512]{4,2,3,0,1:T(4,128)S(1)}) fusion(f32[12,4,512]{2,1,0:T(4,128)S(1)} %copy-done.5, f32[12,4]{1,0:T(8,128)S(1)} %select_reduce_fusion, f32[12,4,4]{1,2,0:T(4,128)S(1)} %copy.78, bf16[12,4,4,128]{3,2,1,0:T(4,128)(2,1)S(1)} %reshape.325, bf16[12,512,1,128]{3,1,2,0:T(8,128)(2,1)} %param.32, ...), kind=kOutput, calls=%fused_computation.119 | convolution fusion | flops 25755456 | bytes 2121408 | tf_op jit(solution)/shard_map/stkgd,spkd->skgtp/dot_general | solution.py:187
  47.7 0.3 fusion.77
  48.4 0.6 copy.75
  49.2 5.1 %all-to-all-start.2 = ((f32[4,16,4]{1,2,0:T(4,128)}), f32[4,16,4]{1,2,0:T(4,128)S(1)}, u32[]{:S(2)}, u32[]{:S(2)}) async-start(f32[4,16,4]{1,2,0:T(4,128)} %copy.75), calls=%async_computation.2 | async-start | bytes 16384 | tf_op jit(solution)/shard_map/all_to_all | solution.py:139
  54.3 1.8 %fusion.65 = bf16[12,4,1,4,128]{4,1,3,0,2:T(4,128)(2,1)S(1)} fusion(f32[12,4,4,128]{3,2,1,0:T(4,128)S(1)} %convolution_multiply_fusion.2, bf16[12,512,1,128]{3,1,2,0:T(8,128)(2,1)} %param.33, bf16[12,4,4,512]{3,1,2,0:T(4,128)(2,1)S(1)} %get-tuple-element.191, f32[12,4,4]{2,1,0:T(4,128)S(1)} %copy.84), kind=kOutput, calls=%fused_computation.59 | convolution fusion | flops 25239552 | bytes 1917696 | tf_op jit(solution)/shard_map/skgtp,spkd->skgtd/dot_general | solution.py:198
  56.0 0.7 copy.72
  56.8 3.2 %all-to-all-done.2 = f32[4,16,4]{1,2,0:T(4,128)S(1)} async-done(((f32[4,16,4]{1,2,0:T(4,128)}), f32[4,16,4]{1,2,0:T(4,128)S(1)}, u32[]{:S(2)}, u32[]{:S(2)}) %all-to-all-start.2) | async-done | bytes 1056 | tf_op jit(solution)/shard_map/all_to_all | solution.py:139
  60.0 3.3 %all-to-all-start = ((f32[4,16,4,128]{3,1,2,0:T(8,128)}), f32[4,16,4,128]{3,1,2,0:T(8,128)S(1)}, u32[]{:S(2)}, u32[]{:S(2)}) async-start(f32[4,16,4,128]{3,1,2,0:T(8,128)} %copy.72), calls=%async_computation | async-start | bytes 262144 | tf_op jit(solution)/shard_map/all_to_all | solution.py:125
  63.3 5.9 %all-to-all-done = f32[4,16,4,128]{3,1,2,0:T(8,128)S(1)} async-done(((f32[4,16,4,128]{3,1,2,0:T(8,128)}), f32[4,16,4,128]{3,1,2,0:T(8,128)S(1)}, u32[]{:S(2)}, u32[]{:S(2)}) %all-to-all-start) | async-done | bytes 131104 | tf_op jit(solution)/shard_map/all_to_all | solution.py:125
  69.4 0.5 convolution_convert_fusion
  69.9 2.2 %all-gather = bf16[128,2048]{1,0:T(8,128)(2,1)S(1)} all-gather(bf16[64,2048]{1,0:T(8,128)(2,1)S(1)} %convolution_convert_fusion), channel_id=2, replica_groups=mesh['dp'=4,'kv'=4,'tp'=2] {'tp'}, dimensions={0}, use_global_device_ids=true | all-gather | bytes 786432 | tf_op jit(solution)/shard_map/all_gather | solution.py:10
  72.5 0.6 slice.51
  73.1 0.8 %reshape.331 = bf16[12,4,2048]{2,1,0:T(4,128)(2,1)} reshape(bf16[48,2048]{1,0:T(8,128)(2,1)S(1)} %slice.52) | data formatting | bytes 393216 | tf_op jit(solution)/shard_map/reshape | solution.py:216
  (115 shorter events, 6.1 us)
Async XLA Ops:
  0.6 68.7 %copy-start = (bf16[512,2048]{1,0:T(8,128)(2,1)S(1)}, bf16[512,2048]{1,0:T(8,128)(2,1)}, u32[]{:S(2)}) copy-start(bf16[512,2048]{1,0:T(8,128)(2,1)} %param.27) | copy-start | bytes 6291460
  0.6 19.8 %copy-start.4 = (bf16[16,2048]{1,0:T(8,128)(2,1)S(1)}, bf16[16,2048]{1,0:T(8,128)(2,1)}, u32[]{:S(2)}) copy-start(bf16[16,2048]{1,0:T(8,128)(2,1)} %param.19) | copy-start | bytes 196612
  0.7 19.8 %copy-start.7 = (f32[2048]{0:T(1024)S(1)}, f32[2048]{0:T(1024)}, u32[]{:S(2)}) copy-start(f32[2048]{0:T(1024)} %param.21) | copy-start | bytes 24580
  0.7 19.8 %copy-start.10 = (bf16[2048,128]{1,0:T(8,128)(2,1)S(1)}, bf16[2048,128]{1,0:T(8,128)(2,1)}, u32[]{:S(2)}) copy-start(bf16[2048,128]{1,0:T(8,128)(2,1)} %param.24) | copy-start | bytes 1572868
  18.2 2.6 %copy-start.1 = (bf16[2048,512]{1,0:T(8,128)(2,1)S(1)}, bf16[2048,512]{1,0:T(8,128)(2,1)}, u32[]{:S(2)}) copy-start(bf16[2048,512]{1,0:T(8,128)(2,1)} %param.22) | copy-start | bytes 6291460
  20.5 14.2 %copy-start.2 = (bf16[256,1,128]{2,0,1:T(8,128)(2,1)S(1)}, bf16[256,1,128]{2,0,1:T(8,128)(2,1)}, u32[]{:S(2)}) copy-start(bf16[256,1,128]{2,0,1:T(8,128)(2,1)} %param.29) | copy-start | bytes 196612
  20.5 14.2 %copy-start.3 = (bf16[256,1,128]{2,0,1:T(8,128)(2,1)S(1)}, bf16[256,1,128]{2,0,1:T(8,128)(2,1)}, u32[]{:S(2)}) copy-start(bf16[256,1,128]{2,0,1:T(8,128)(2,1)} %param.30) | copy-start | bytes 196612
  20.8 22.5 %copy-start.6 = (bf16[64,128]{1,0:T(8,128)(2,1)}, bf16[64,128]{1,0:T(8,128)(2,1)S(1)}, u32[]{:S(2)}) copy-start(bf16[64,128]{1,0:T(8,128)(2,1)S(1)} %convolution_convert_fusion.2) | copy-start | bytes 49156
  21.4 21.8 %copy-start.9 = (s32[12]{0:T(128)S(1)}, s32[12]{0:T(128)}, u32[]{:S(2)}) copy-start(s32[12]{0:T(128)} %param.35) | copy-start | bytes 148
  34.6 10.8 %copy-start.5 = (f32[12,4,512]{2,1,0:T(4,128)S(1)}, f32[12,4,512]{2,1,0:T(4,128)}, u32[]{:S(2)}) copy-start(f32[12,4,512]{2,1,0:T(4,128)} %param.34) | copy-start | bytes 294916
  39.7 9.4 %all-to-all-start.1 = ((f32[4,16,4]{1,2,0:T(4,128)}), f32[4,16,4]{1,2,0:T(4,128)S(1)}, u32[]{:S(2)}, u32[]{:S(2)}) async-start(f32[4,16,4]{1,2,0:T(4,128)} %copy.73), calls=%async_computation.1 | async-start | bytes 16384 | tf_op jit(solution)/shard_map/all_to_all | solution.py:132
  43.5 4.6 %slice-start = ((bf16[64,128]{1,0:T(8,128)(2,1)}), bf16[48,128]{1,0:T(8,128)(2,1)S(1)}, s32[]{:S(2)}) async-start(bf16[64,128]{1,0:T(8,128)(2,1)} %copy-done.6), calls=%async_computation.3 | async-start | bytes 24576 | tf_op jit(solution)/shard_map/slice | solution.py:154
  49.2 10.8 %all-to-all-start.2 = ((f32[4,16,4]{1,2,0:T(4,128)}), f32[4,16,4]{1,2,0:T(4,128)S(1)}, u32[]{:S(2)}, u32[]{:S(2)}) async-start(f32[4,16,4]{1,2,0:T(4,128)} %copy.75), calls=%async_computation.2 | async-start | bytes 16384 | tf_op jit(solution)/shard_map/all_to_all | solution.py:139
  60.0 9.2 %all-to-all-start = ((f32[4,16,4,128]{3,1,2,0:T(8,128)}), f32[4,16,4,128]{3,1,2,0:T(8,128)S(1)}, u32[]{:S(2)}, u32[]{:S(2)}) async-start(f32[4,16,4,128]{3,1,2,0:T(8,128)} %copy.72), calls=%async_computation | async-start | bytes 262144 | tf_op jit(solution)/shard_map/all_to_all | solution.py:125
  69.4 3.0 %copy-start.8 = (f32[2048]{0:T(1024)S(1)}, f32[2048]{0:T(1024)}, u32[]{:S(2)}) copy-start(f32[2048]{0:T(1024)} %param.28) | copy-start | bytes 24580
